TPU v7x, 32 devices: a whole 2x2x4 slice. The times are simulated.
32 devices in a mesh: sp: 8 (over z, y), tp: 4 (over x, core).
Axes of the slice: x: 2, y: 2, z: 4, core: 2. Of those that a mesh axis runs over, the one named last changes fastest.
Arguments:
- inputs: bfloat16 [2, 1024, 2048], P(None, 'sp'), may hold values from -6 to 6
- norm_gain: float32 [2048], replicated, may hold values from 0.1 to 1.9
- query_weight: bfloat16 [2048, 1024], P('sp', 'tp'), may hold values from -0.125 to 0.125
- key_weight: bfloat16 [2048, 256], P('sp', 'tp'), may hold values from -0.125 to 0.125
- value_weight: bfloat16 [2048, 256], P('sp', 'tp'), may hold values from -0.125 to 0.125
- query_gain: float32 [64], replicated, may hold values from 0.1 to 24
- key_gain: float32 [64], replicated, may hold values from 0.1 to 1.9
- forget_cache: float32 [2, 16, 1024], P(None, 'tp'), may hold values from -104 to 0, as said below
- rec_in_weight: bfloat16 [2048, 1024], P('sp', 'tp'), may hold values from -0.125 to 0.125
- rec_gate_weight: bfloat16 [2048, 1024], P('sp', 'tp'), may hold values from -0.125 to 0.125
- conv_weight: bfloat16 [4, 1024], P(None, 'tp'), may hold values from -3 to 3
- decay_gate_weight: bfloat16 [16, 64, 64], P('tp'), may hold values from -0.75 to 0.75
- input_gate_weight: bfloat16 [16, 64, 64], P('tp'), may hold values from -0.75 to 0.75
- decay_param: float32 [1024], P('tp'), may hold values from 4 to 16
- decay_extra: float32 [2, 1024, 1024], P(None, 'sp', 'tp'), may hold values from -2 to 0
- attn_out_gain: float32 [1024], P('tp'), may hold values from 0.1 to 1.9
- rec_out_gain: float32 [1024], P('tp'), may hold values from 0.1 to 1.9
- out_att_weight: bfloat16 [1024, 2048], P('tp'), may hold values from -0.125 to 0.125
- out_rec_weight: bfloat16 [1024, 2048], P('tp'), may hold values from -0.125 to 0.125
Outputs:
- mixed: bfloat16 [2, 1024, 2048], P(None, 'sp', 'tp')
Inputs may be any that keep to these rules, and one draw needn't show every extreme that they name: `forget_cache`: Non-increasing along the positions of each sequence and head.
All inputs are finite; a program needn't handle non-finite values.
Results may differ from a plain program's by a relative error of at most 0.012.
The roundings to bfloat16 on the way count: a program that leaves them out, or rounds other values in their place, can miss the bound.
Values may be sent and summed in bfloat16 or wider, within the bound.
A program may use at most 128 MiB of HBM per device.

v0:
```python
import jax
import jax.numpy as jnp
from jax import lax
from jax.sharding import PartitionSpec as P

D = 2048
LRU_BLOCK = 64
CONV_TAPS = 4
lru_const = 8.0
norm_eps = 1e-06


def from_behind(value, axis, steps):
    count = lax.axis_size(axis)
    leading, last = (max(0, -steps), min(count, count - steps))
    return lax.ppermute(value, axis, [(source, source + steps) for source in range(leading, last)])


def rms_scale(values, gain):
    multiplier = lax.rsqrt(jnp.mean(values * values, axis=-1, keepdims=True) + norm_eps)
    return values * multiplier * gain


def merge_state(earlier, later):
    return (earlier[0] * later[0], later[0] * earlier[1] + later[1])


def block_length(length, span):
    shards = max(length // span, 1)
    group_size = 1
    for trial_size in range(1, shards + 1):
        if shards % trial_size == 0 and trial_size * span <= 1024:
            group_size = trial_size
    sub_size = group_size * span
    if length % sub_size:
        sub_size = length
    return sub_size


def body(
    inputs,
    norm_gain,
    query_weight,
    key_weight,
    value_weight,
    query_gain,
    key_gain,
    forget_cache,
    rec_in_weight,
    rec_gate_weight,
    conv_weight,
    decay_gate_weight,
    input_gate_weight,
    decay_param,
    decay_extra,
    attn_out_gain,
    rec_out_gain,
    out_att_weight,
    out_rec_weight,
):
    seq_count, seq_span, model_width = inputs.shape
    row_count = seq_count * seq_span
    head_dim = query_gain.shape[0]
    att_local = query_weight.shape[1] // head_dim
    kv_local = key_weight.shape[1] // head_dim
    head_group = att_local // kv_local
    channels = rec_in_weight.shape[1]
    normed = rms_scale(
        inputs.reshape(row_count, model_width).astype(jnp.float32), norm_gain
    ).astype(jnp.bfloat16)
    normed_cols = normed.T
    row_contract = (((0,), (0,)), ((), ()))
    kv_cols = key_weight.shape[1]
    pieces = (
        lax.all_gather(query_weight, "sp", axis=0, tiled=True),
        lax.all_gather(key_weight, "sp", axis=0, tiled=True),
        lax.all_gather(value_weight, "sp", axis=0, tiled=True),
        lax.all_gather(rec_in_weight, "sp", axis=0, tiled=True),
        lax.all_gather(rec_gate_weight, "sp", axis=0, tiled=True),
    )
    query_proj, key_proj, value_sum, rec_in_sum, gate_proj = tuple(
        (
            lax.dot_general(
                normed_cols, weight_part, row_contract, preferred_element_type=jnp.float32
            )
            for weight_part in pieces
        )
    )
    queries = rms_scale(query_proj.reshape(row_count, att_local, head_dim), query_gain).astype(
        jnp.bfloat16
    )
    queries = queries.reshape(seq_count, seq_span, kv_local, head_group, head_dim).transpose(
        0, 2, 3, 1, 4
    )
    queries = queries.reshape(seq_count, kv_local, head_group * seq_span, head_dim)
    key_heads = rms_scale(key_proj.reshape(row_count, kv_local, head_dim), key_gain).astype(
        jnp.bfloat16
    )
    key_heads = key_heads.reshape(seq_count, seq_span, kv_cols)
    value_heads = value_sum.astype(jnp.bfloat16).reshape(seq_count, seq_span, kv_cols)
    key_value = jnp.concatenate([key_heads, value_heads], axis=2)
    my_first = lax.axis_index("sp") * seq_span
    own_gates = lax.dynamic_slice_in_dim(forget_cache, my_first, seq_span, 2)
    own_gates = own_gates.reshape(seq_count, kv_local, head_group, seq_span, 1)
    query_pos = my_first + jnp.tile(jnp.arange(seq_span, dtype=jnp.int32), head_group)
    scaling = head_dim ** (-0.5)
    start_state = (
        jnp.full((seq_count, kv_local, head_group * seq_span), -jnp.inf, jnp.float32),
        jnp.zeros((seq_count, kv_local, head_group * seq_span), jnp.float32),
        jnp.zeros((seq_count, kv_local, head_group * seq_span, head_dim), jnp.float32),
    )
    shard_part = lax.all_gather(key_value, "sp", axis=1, tiled=True)
    offset = jnp.int32(0)
    length = shard_part.shape[1]
    sub_size = block_length(length, seq_span)

    def one_step(block_index, carried_state):
        key_first = offset + block_index * sub_size

        def work(carried):
            top_score, totals, accum = carried
            block_rows = lax.dynamic_slice_in_dim(shard_part, block_index * sub_size, sub_size, 1)
            key_block = block_rows[:, :, :kv_cols].reshape(seq_count, sub_size, kv_local, head_dim)
            value_block = block_rows[:, :, kv_cols:].reshape(
                seq_count, sub_size, kv_local, head_dim
            )
            key_gates = lax.dynamic_slice_in_dim(forget_cache, key_first, sub_size, 2)
            key_gates = key_gates.reshape(seq_count, kv_local, head_group, 1, sub_size)
            scores = (
                jnp.einsum(
                    "bhqd,bkhd->bhqk", queries, key_block, preferred_element_type=jnp.float32
                )
                * scaling
            )
            scores = (
                scores.reshape(seq_count, kv_local, head_group, seq_span, sub_size)
                + own_gates
                - key_gates
            )
            scores = scores.reshape(seq_count, kv_local, head_group * seq_span, sub_size)
            visible = (
                query_pos[:, None] >= (key_first + jnp.arange(sub_size, dtype=jnp.int32))[None, :]
            )
            scores = jnp.where(visible, scores, -jnp.inf)
            new_top = jnp.maximum(top_score, jnp.max(scores, axis=-1))
            safe_top = jnp.where(jnp.isfinite(new_top), new_top, 0.0)
            weights = jnp.exp(scores - safe_top[..., None])
            fading = jnp.exp(top_score - safe_top)
            totals = totals * fading + jnp.sum(weights, axis=-1)
            accum = accum * fading[..., None] + jnp.einsum(
                "bhqk,bkhd->bhqd",
                weights.astype(jnp.bfloat16),
                value_block,
                preferred_element_type=jnp.float32,
            )
            return (new_top, totals, accum)

        return lax.cond(
            key_first < my_first + seq_span, work, lambda carried: carried, carried_state
        )

    top_score, totals, accum = lax.fori_loop(0, length // sub_size, one_step, start_state)
    attended = (accum / totals[..., None]).reshape(
        seq_count, kv_local, head_group, seq_span, head_dim
    )
    attended = attended.transpose(0, 3, 1, 2, 4).reshape(row_count, att_local, head_dim)
    att_normed = rms_scale(attended, attn_out_gain.reshape(att_local, head_dim)).astype(
        jnp.bfloat16
    )
    att_normed = att_normed.reshape(row_count, att_local * head_dim)
    rec_in = rec_in_sum.astype(jnp.bfloat16).reshape(seq_count, seq_span, channels)
    before = from_behind(rec_in[:, seq_span - (CONV_TAPS - 1) :, :], "sp", 1)
    extended = jnp.concatenate([before, rec_in], axis=1)
    conv = jnp.zeros((seq_count, seq_span, channels), jnp.float32)
    for tap in range(CONV_TAPS):
        conv = conv + extended[:, tap : tap + seq_span].astype(jnp.float32) * conv_weight[
            tap
        ].astype(jnp.float32)
    conv = conv.astype(jnp.bfloat16)
    blocks_local = decay_gate_weight.shape[0]
    grouped = conv.reshape(seq_count, seq_span, blocks_local, LRU_BLOCK)
    gate_decay = jnp.einsum(
        "bsnd,nde->bsne", grouped, decay_gate_weight, preferred_element_type=jnp.float32
    ).reshape(seq_count, seq_span, channels)
    gate_input = jnp.einsum(
        "bsnd,nde->bsne", grouped, input_gate_weight, preferred_element_type=jnp.float32
    ).reshape(seq_count, seq_span, channels)
    log_decay = (
        -lru_const * jax.nn.sigmoid(gate_decay) * jax.nn.softplus(-decay_param) + decay_extra
    )
    drive = (
        jnp.sqrt(-jnp.expm1(2.0 * log_decay))
        * jax.nn.sigmoid(gate_input)
        * conv.astype(jnp.float32)
    )
    cum_decay, local_state = lax.associative_scan(merge_state, (jnp.exp(log_decay), drive), axis=1)
    every_decay, every_state = (
        lax.all_gather(cum_decay[:, seq_span - 1][None], "sp", axis=0, tiled=True),
        lax.all_gather(local_state[:, seq_span - 1][None], "sp", axis=0, tiled=True),
    )
    prefix_decay, prefix_state = lax.associative_scan(
        merge_state, (every_decay, every_state), axis=0
    )
    position = lax.axis_index("sp")
    earlier_state = lax.dynamic_index_in_dim(
        prefix_state, jnp.maximum(position - 1, 0), 0, keepdims=False
    )
    entering = jnp.where(position > 0, earlier_state, 0.0)
    state = local_state + cum_decay * entering[:, None, :]
    gated = state * jax.nn.gelu(gate_proj.reshape(seq_count, seq_span, channels))
    rec_normed = rms_scale(
        gated.reshape(row_count, blocks_local, LRU_BLOCK),
        rec_out_gain.reshape(blocks_local, LRU_BLOCK),
    ).astype(jnp.bfloat16)
    rec_normed = rec_normed.reshape(row_count, channels)
    out_cols = D // lax.axis_size("tp")
    pieces = row_count * lax.axis_size("tp") // row_count
    terms = jnp.dot(att_normed, out_att_weight, preferred_element_type=jnp.float32) + jnp.dot(
        rec_normed, out_rec_weight, preferred_element_type=jnp.float32
    )
    mixed_cols = lax.psum_scatter(
        terms.reshape(row_count, pieces, out_cols)
        .transpose(1, 0, 2)
        .reshape(pieces * row_count, out_cols)
        .astype(jnp.bfloat16),
        "tp",
        scatter_dimension=0,
        tiled=True,
    )
    return mixed_cols.reshape(seq_count, seq_span, out_cols)


def solution(mesh):
    return jax.shard_map(
        body,
        mesh=mesh,
        in_specs=(
            P(None, "sp", None),
            P(),
            P("sp", "tp"),
            P("sp", "tp"),
            P("sp", "tp"),
            P(),
            P(),
            P(None, "tp", None),
            P("sp", "tp"),
            P("sp", "tp"),
            P(None, "tp"),
            P("tp", None, None),
            P("tp", None, None),
            P("tp"),
            P(None, "sp", "tp"),
            P("tp"),
            P("tp"),
            P("tp", None),
            P("tp", None),
        ),
        out_specs=P(None, "sp", "tp"),
        check_vma=False,
    )
```

profile of v0, /device:TPU:0, one launch (start us, length us, event | category | flops | bytes accessed | tf_op | source)
XLA Modules:
  0.0 263.9 jit_solution(10849590766930557368)
XLA Ops:
  9.5 1.5 multiply_reduce_fusion
  11.0 1.4 slice_convert_fusion.3
  12.4 33.4 %all_gather.25 = bf16[2048,64]{0,1:T(8,128)(2,1)S(1)} all-gather(bf16[256,64]{0,1:T(8,128)(2,1)} %param.24), channel_id=1, replica_groups=mesh['sp'=8,'tp'=4] {'sp'}, dimensions={0}, use_global_device_ids=true | all-gather | bytes 294912 | tf_op jit(solution)/shard_map/all_gather | solution.py:76
  45.8 31.4 %all_gather.26 = bf16[2048,64]{0,1:T(8,128)(2,1)S(1)} all-gather(bf16[256,64]{0,1:T(8,128)(2,1)} %param.25), channel_id=1, replica_groups=mesh['sp'=8,'tp'=4] {'sp'}, dimensions={0}, use_global_device_ids=true | all-gather | bytes 294912 | tf_op jit(solution)/shard_map/all_gather | solution.py:77
  77.2 1.0 fusion.14
  79.3 29.7 %all_gather.27 = bf16[2,1024,128]{1,2,0:T(8,128)(2,1)} all-gather(bf16[2,128,128]{1,2,0:T(8,128)(2,1)S(1)} %pad_maximum_fusion.3), channel_id=1, replica_groups=mesh['sp'=8,'tp'=4] {'sp'}, dimensions={1}, use_global_device_ids=true | all-gather | bytes 589824 | tf_op jit(solution)/shard_map/all_gather | solution.py:112
  108.9 1.3 multiply_convert_fusion
  110.3 2.4 copy.49
  112.6 1.7 multiply_reduce_fusion.1
  114.6 6.3 %conditional.1 = ((f32[2,1,512]{2,0,1:T(2,128)S(1)}, f32[2,1,512,64]{2,3,0,1:T(8,128)S(1)})) conditional(s32[]{:T(128)} %convert_element_type.124, (f32[2,1,512]{2,0,1:T(2,128)S(1)}, f32[2,1,512,64]{2,3,0,1:T(8,128)S(1)}) %tuple.30, (s32[]{:T(128)}, s32[4,128]{1,0:T(4,128)S(1)}, bf16[2,1,4,128,64]{3,2,4,0,1:T(4,128)(2,1)S(1)}, ...), branch_computations={%region_3.4_spmd, %region_4.7_spmd} | conditional | flops 281680384 | bytes 17967226 | solution.py:158
  114.7 0.8 dynamic-slice_bitcast_fusion
  115.9 2.4 fusion.3
  118.4 1.8 fusion.1
  120.2 0.8 fusion.4
  121.5 1.7 convolution_convert_fusion
  123.3 3.3 %collective-permute-start = (bf16[2,3,256]{2,1,0:T(4,128)(2,1)S(1)}, bf16[2,3,256]{2,1,0:T(4,128)(2,1)S(1)}, u32[]{:S(2)}, u32[]{:S(2)}) collective-permute-start(bf16[2,3,256]{2,1,0:T(4,128)(2,1)S(1)} %slice.399), channel_id=1, source_target_pairs={{0,4},{4,8},{8,12},{12,16},{16,20},{20,24},{24,28},{1,5},{5,9},{9,... | collective-permute-start | bytes 9224 | tf_op jit(solution)/shard_map/ppermute | solution.py:16
  129.1 0.8 copy.62
  129.9 1.2 fusion.22
  131.1 0.8 copy.58
  132.0 2.0 convert_multiply_fusion
  134.7 1.6 slice.363
  136.4 1.0 slice.317
  137.3 1.6 slice.316
  141.6 1.1 multiply_add_fusion.1
  147.7 0.8 fusion.53
  149.2 0.8 pad.128
  151.9 0.9 pad_maximum_fusion.4
  152.8 2.1 pad.116
  154.9 0.8 pad.130
  155.7 1.6 add.383
  157.3 1.7 fusion.45
  159.0 1.5 pad.117
  160.5 2.3 pad.118
  162.8 0.7 slice_add_fusion.4
  163.6 26.3 %all-gather = f32[16,1,256]{2,1,0:T(1,128)S(1)} all-gather(f32[2,1,256]{2,1,0:T(1,128)S(1)} %slice_add_fusion.4), channel_id=2, replica_groups=mesh['sp'=8,'tp'=4] {'sp'}, dimensions={0}, use_global_device_ids=true | all-gather | bytes 18432 | tf_op jit(solution)/shard_map/all_gather | solution.py:199
  190.4 1.6 pad_maximum_fusion.2
  192.0 0.9 pad.131
  193.6 0.7 reshape.378
  194.3 1.2 copy.63
  195.6 1.4 pad.132
  197.7 26.1 %all-gather.1 = f32[16,1,256]{2,1,0:T(1,128)S(1)} all-gather(f32[2,1,256]{2,1,0:T(1,128)S(1)} %slice_add_fusion.3), channel_id=3, replica_groups=mesh['sp'=8,'tp'=4] {'sp'}, dimensions={0}, use_global_device_ids=true | all-gather | bytes 18432 | tf_op jit(solution)/shard_map/all_gather | solution.py:198
  224.9 3.0 %fusion.73 = (f32[2,128,256]{2,1,0:T(8,128)}, f32[2,128,256]{2,1,0:T(8,128)}) fusion(bf16[2,128,2048]{2,1,0:T(8,128)(2,1)} %multiply_convert_fusion, bf16[2048,256]{1,0:T(8,128)(2,1)} %all-gather.10.cloned.1.call-done, f32[2,256]{1,0:T(2,128)S(1)} %fusion.65, f32[2,128,256]{2,1,0:T(8,128)S(1)} %pad.131, f32[2,128,256]{2,1,0:T(8,128)} %pad.132, ...), kind=kOutput, calls=%fused_computation.170 | convolution fusion | flops 269352960 | bytes 3672064 | tf_op jit(solution)/shard_map/dot_general | solution.py:83
  227.9 1.8 copy.64
  229.7 1.2 mul.431
  230.9 1.1 copy.65
  232.1 1.7 fusion.12
  233.8 1.1 copy.94
  234.9 22.5 %reduce-scatter.2.cloned.1.call-done = bf16[256,512]{1,0:T(8,128)(2,1)} async-done(((bf16[1024,512]{1,0:T(8,128)(2,1)}), bf16[256,512]{1,0:T(8,128)(2,1)}) %reduce-scatter.2.cloned.1.call-update) | async-done | bytes 262160 | tf_op jit(solution)/shard_map/reduce_scatter | solution.py:221
  (192 shorter events, 21.6 us)
Async XLA Ops:
  6.5 120.2 %copy-start = (bf16[256,2048]{1,0:T(8,128)(2,1)S(1)}, bf16[256,2048]{1,0:T(8,128)(2,1)}, u32[]{:S(2)}) copy-start(bf16[256,2048]{1,0:T(8,128)(2,1)} %param.38) | copy-start | bytes 3145732
  6.5 70.7 %copy-start.1 = (bf16[2,128,2048]{2,1,0:T(8,128)(2,1)S(1)}, bf16[2,128,2048]{2,1,0:T(8,128)(2,1)}, u32[]{:S(2)}) copy-start(bf16[2,128,2048]{2,1,0:T(8,128)(2,1)} %param.21) | copy-start | bytes 3145732
  6.5 103.7 %all-gather.6.cloned.1.call-start = ((), (), s32[]{:S(2)}) async-start(), calls=%async_computation.1 | async-start | bytes 1179648 | tf_op jit(solution)/shard_map/all_gather | solution.py:75
  7.3 114.3 %all-gather.8.cloned.1.call-start = ((), (), s32[]{:S(2)}) async-start(), calls=%async_computation.2 | async-start | bytes 1179648 | tf_op jit(solution)/shard_map/all_gather | solution.py:78
  8.0 216.8 %all-gather.10.cloned.1.call-start = ((), (), s32[]{:S(2)}) async-start(), calls=%async_computation.3 | async-start | bytes 1179648 | tf_op jit(solution)/shard_map/all_gather | solution.py:79
  8.7 248.6 %reduce-scatter.2.cloned.1.call-start = ((), (), s32[]{:S(2)}) async-start(), calls=%async_computation.4 | async-start | bytes 1310720 | tf_op jit(solution)/shard_map/reduce_scatter | solution.py:221
  77.2 2.0 copy-start.15
  78.2 30.7 %copy-start.8 = (f32[2048]{0:T(1024)S(1)}, f32[2048]{0:T(1024)}, u32[]{:S(2)}) copy-start(f32[2048]{0:T(1024)} %param.22) | copy-start | bytes 24580
  110.2 2.4 copy-start.2
  112.6 1.7 copy-start.16
  115.9 2.5 copy-start.6
  118.3 1.8 copy-start.3
  121.0 5.6 %copy-start.13 = (f32[256]{0:T(256)S(1)}, f32[256]{0:T(256)}, u32[]{:S(2)}) copy-start(f32[256]{0:T(256)} %param.36) | copy-start | bytes 3076
  123.2 4.6 %copy-start.9 = (f32[1,256]{1,0:T(1,128)S(1)}, f32[1,256]{1,0:T(1,128)}, u32[]{:S(2)}) copy-start(f32[1,256]{1,0:T(1,128)} %get-tuple-element.199) | copy-start | bytes 3076
  123.2 4.6 %copy-start.10 = (f32[1,256]{1,0:T(1,128)S(1)}, f32[1,256]{1,0:T(1,128)}, u32[]{:S(2)}) copy-start(f32[1,256]{1,0:T(1,128)} %get-tuple-element.200) | copy-start | bytes 3076
  123.2 4.6 %copy-start.11 = (f32[1,256]{1,0:T(1,128)S(1)}, f32[1,256]{1,0:T(1,128)}, u32[]{:S(2)}) copy-start(f32[1,256]{1,0:T(1,128)} %get-tuple-element.201) | copy-start | bytes 3076
  123.2 4.6 %copy-start.12 = (f32[1,256]{1,0:T(1,128)S(1)}, f32[1,256]{1,0:T(1,128)}, u32[]{:S(2)}) copy-start(f32[1,256]{1,0:T(1,128)} %get-tuple-element.202) | copy-start | bytes 3076
  123.3 4.6 %collective-permute-start = (bf16[2,3,256]{2,1,0:T(4,128)(2,1)S(1)}, bf16[2,3,256]{2,1,0:T(4,128)(2,1)S(1)}, u32[]{:S(2)}, u32[]{:S(2)}) collective-permute-start(bf16[2,3,256]{2,1,0:T(4,128)(2,1)S(1)} %slice.399), channel_id=1, source_target_pairs={{0,4},{4,8},{8,12},{12,16},{16,20},{20,24},{24,28},{1,5},{5,9},{9,... | collective-permute-start | bytes 9224 | tf_op jit(solution)/shard_map/ppermute | solution.py:16
  126.6 2.2 copy-start.17
  128.1 0.7 copy-start.7
  144.1 7.1 %copy-start.4 = (f32[2,31,256]{2,1,0:T(8,128)S(1)}, f32[2,31,256]{2,1,0:T(8,128)}, u32[]{:S(2)}) copy-start(f32[2,31,256]{2,1,0:T(8,128)} %slice.361) | copy-start | bytes 190468
  144.2 7.1 %copy-start.5 = (f32[2,31,256]{2,1,0:T(8,128)S(1)}, f32[2,31,256]{2,1,0:T(8,128)}, u32[]{:S(2)}) copy-start(f32[2,31,256]{2,1,0:T(8,128)} %slice.320) | copy-start | bytes 190468
  224.8 7.1 %copy-start.14 = (f32[256]{0:T(256)S(1)}, f32[256]{0:T(256)}, u32[]{:S(2)}) copy-start(f32[256]{0:T(256)} %param.37) | copy-start | bytes 3076
Sparse Core Ops, SparseCore 0:
  9.5 44.2 all-gather.5
  55.9 41.5 all-gather.7
  99.6 38.9 all-gather.9
  235.0 22.3 reduce-scatter.1
where the time goes:
time: 265 us; the launch traced here: 264 us
  blocking collectives  147 us (55%)
  local copies, waits for them, and re-layouts  35.4 us (13%)
  waiting for transfers between devices  25.4 us (10%)
  other arithmetic  24.8 us (9%)
  matrix products  14.1 us (5%)
  between operations  13.9 us (5%)
  starting transfers between devices  3.38 us (1%)
    all_gather x1, blocking collectives, body(): lax.all_gather(key_weight, 'sp', axis=0, tiled=True)  33.4 us
    all_gather x1, blocking collectives, body(): lax.all_gather(value_weight, 'sp', axis=0, tiled=True)  31.4 us
    all_gather x1, blocking collectives, body(): shard_part = lax.all_gather(key_value, 'sp', axis=1, tiled=True)  29.7 us
    all_gather x1, blocking collectives, body(): lax.all_gather(local_state[:, seq_span - 1][None], 'sp', axis=0, tiled=True)  26.3 us
    all_gather x1, blocking collectives, body(): lax.all_gather(cum_decay[:, seq_span - 1][None], 'sp', axis=0, tiled=True)  26.1 us
    reduce_scatter x1, waiting for transfers between devices, body(): lax.psum_scatter(terms.reshape(row_count, pieces, out_cols).transpose(1,...  22.5 us
    slice x44, local copies, waits for them, and re-layouts, body(): lax.associative_scan(merge_state, (jnp.exp(log_decay), drive), axis=1)  11.2 us
    pad x24, local copies, waits for them, and re-layouts, body(): lax.associative_scan(merge_state, (jnp.exp(log_decay), drive), axis=1)  10.2 us
  transfers between devices with their start and end apart: 5, of which 2 were waited for; matrix products, arithmetic and copies ran while one was open for 24% of the time, Pallas kernels for 0%

commit v1 on v0

--- a/solution.py
+++ b/solution.py
@@ -109,7 +109,12 @@
         jnp.zeros((seq_count, kv_local, head_group * seq_span), jnp.float32),
         jnp.zeros((seq_count, kv_local, head_group * seq_span, head_dim), jnp.float32),
     )
-    shard_part = lax.all_gather(key_value, "sp", axis=1, tiled=True)
+    ring = [key_value]
+    for hop in range(7):
+        ring.append(lax.ppermute(ring[-1], "sp", [(dev, (dev + 1) % 8) for dev in range(8)]))
+    shard_part = jnp.roll(
+        jnp.concatenate(ring[::-1], axis=1), (lax.axis_index("sp") + 1) * ring[0].shape[1], axis=1
+    )
     offset = jnp.int32(0)
     length = shard_part.shape[1]
     sub_size = block_length(length, seq_span)

time: 265 us -> 375 us (1.42)
  local copies, waits for them, and re-layouts: 35.4 us -> 107 us
  waiting for transfers between devices: 25.4 us -> 70.1 us
  blocking collectives: 147 us -> 116 us
  other arithmetic: 24.8 us -> 40.3 us
  matrix products: 14.1 us -> 19.7 us
    ppermute x0 -> x7, waiting for transfers between devices: none -> 46.5 us  [body(): lax.ppermute(ring[-1], 'sp', [(dev, (dev + 1) % 8) for dev in range(8)])]
    slice x44, local copies, waits for them, and re-layouts: 11.2 us -> 51.4 us  [body(): lax.associative_scan(merge_state, (jnp.exp(log_decay), drive), axis=1)]
    all_gather x1 -> x0, blocking collectives: 29.7 us -> none  [body(): shard_part = lax.all_gather(key_value, 'sp', axis=1, tiled=True)]
    unnamed x33 -> x58, local copies, waits for them, and re-layouts: 0.72 us -> 22.8 us
    sub x0 -> x2, local copies, waits for them, and re-layouts: none -> 9.44 us  [work(): scores.reshape(seq_count, kv_local, head_group, seq_span, sub_size)]
    add x13, other arithmetic: 4.34 us -> 13.7 us  [merge_state(): return (earlier[0] * later[0], later[0] * earlier[1] + later[1])]
    concatenate x11, other arithmetic: 3.16 us -> 7.83 us  [body(): lax.associative_scan(merge_state, (jnp.exp(log_decay), drive), axis=1)]
  transfers between devices with their start and end apart: 5 -> 12, of which waited for: 2 -> 8; matrix products, arithmetic and copies ran while one was open for 24% -> 42% of each run, Pallas kernels for 0% -> 0%
where the time goes in v1:
time: 375 us; the launch traced here: 371 us
  blocking collectives  116 us (31%)
  local copies, waits for them, and re-layouts  107 us (29%)
  waiting for transfers between devices  70.1 us (19%)
  other arithmetic  40.3 us (11%)
  matrix products  19.7 us (5%)
  between operations  13.9 us (4%)
    slice x44, local copies, waits for them, and re-layouts, body(): lax.associative_scan(merge_state, (jnp.exp(log_decay), drive), axis=1)  51.4 us
    ppermute x7, waiting for transfers between devices, body(): lax.ppermute(ring[-1], 'sp', [(dev, (dev + 1) % 8) for dev in range(8)])  46.5 us
    all_gather x1, blocking collectives, body(): lax.all_gather(value_weight, 'sp', axis=0, tiled=True)  33.1 us
    all_gather x1, blocking collectives, body(): lax.all_gather(key_weight, 'sp', axis=0, tiled=True)  31 us
    all_gather x1, blocking collectives, body(): lax.all_gather(cum_decay[:, seq_span - 1][None], 'sp', axis=0, tiled=True)  26.1 us
    all_gather x1, blocking collectives, body(): lax.all_gather(local_state[:, seq_span - 1][None], 'sp', axis=0, tiled=True)  26.1 us
    unnamed x58, local copies, waits for them, and re-layouts  22.8 us
    reduce_scatter x1, waiting for transfers between devices, body(): lax.psum_scatter(terms.reshape(row_count, pieces, out_cols).transpose(1,...  22.1 us
  transfers between devices with their start and end apart: 12, of which 8 were waited for; matrix products, arithmetic and copies ran while one was open for 42% of the time, Pallas kernels for 0%

profile of v1, /device:TPU:0, one launch (start us, length us, event | category | flops | bytes accessed | tf_op | source)
XLA Modules:
  0.0 370.7 jit_solution(11870754059117342559)
XLA Ops:
  8.1 1.5 multiply_reduce_fusion
  9.6 33.1 %all_gather.22 = bf16[2048,64]{0,1:T(8,128)(2,1)S(1)} all-gather(bf16[256,64]{0,1:T(8,128)(2,1)} %param.25), channel_id=1, replica_groups=mesh['sp'=8,'tp'=4] {'sp'}, dimensions={0}, use_global_device_ids=true | all-gather | bytes 294912 | tf_op jit(solution)/shard_map/all_gather | solution.py:77
  42.7 1.5 fusion.22
  44.7 31.0 %all_gather.21 = bf16[2048,64]{0,1:T(8,128)(2,1)S(1)} all-gather(bf16[256,64]{0,1:T(8,128)(2,1)S(1)} %copy-done.12), channel_id=1, replica_groups=mesh['sp'=8,'tp'=4] {'sp'}, dimensions={0}, use_global_device_ids=true | all-gather | bytes 294912 | tf_op jit(solution)/shard_map/all_gather | solution.py:76
  76.2 1.6 collective-permute-start
  77.9 5.5 %collective-permute-done = bf16[2,128,128]{1,2,0:T(8,128)(2,1)S(1)} collective-permute-done((bf16[2,128,128]{1,2,0:T(8,128)(2,1)S(1)}, bf16[2,128,128]{1,2,0:T(8,128)(2,1)S(1)}, u32[]{:S(2)}, u32[]{:S(2)}) %collective-permute-start) | collective-permute-done | bytes 65568 | tf_op jit(solution)/shard_map/ppermute | solution.py:114
  83.3 7.6 %collective-permute-done.1 = bf16[2,128,128]{1,2,0:T(8,128)(2,1)S(1)} collective-permute-done((bf16[2,128,128]{1,2,0:T(8,128)(2,1)S(1)}, bf16[2,128,128]{1,2,0:T(8,128)(2,1)S(1)}, u32[]{:S(2)}, u32[]{:S(2)}) %collective-permute-start.1) | collective-permute-done | bytes 65568 | tf_op jit(solution)/shard_map/ppermute | solution.py:114
  90.9 7.0 %collective-permute-done.2 = bf16[2,128,128]{1,2,0:T(8,128)(2,1)S(1)} collective-permute-done((bf16[2,128,128]{1,2,0:T(8,128)(2,1)S(1)}, bf16[2,128,128]{1,2,0:T(8,128)(2,1)S(1)}, u32[]{:S(2)}, u32[]{:S(2)}) %collective-permute-start.2) | collective-permute-done | bytes 65568 | tf_op jit(solution)/shard_map/ppermute | solution.py:114
  98.0 6.9 %collective-permute-done.3 = bf16[2,128,128]{1,2,0:T(8,128)(2,1)S(1)} collective-permute-done((bf16[2,128,128]{1,2,0:T(8,128)(2,1)S(1)}, bf16[2,128,128]{1,2,0:T(8,128)(2,1)S(1)}, u32[]{:S(2)}, u32[]{:S(2)}) %collective-permute-start.3) | collective-permute-done | bytes 65568 | tf_op jit(solution)/shard_map/ppermute | solution.py:114
  106.2 5.8 %collective-permute-done.4 = bf16[2,128,128]{1,2,0:T(8,128)(2,1)S(1)} collective-permute-done((bf16[2,128,128]{1,2,0:T(8,128)(2,1)S(1)}, bf16[2,128,128]{1,2,0:T(8,128)(2,1)S(1)}, u32[]{:S(2)}, u32[]{:S(2)}) %collective-permute-start.4) | collective-permute-done | bytes 65568 | tf_op jit(solution)/shard_map/ppermute | solution.py:114
  113.2 6.7 %collective-permute-done.5 = bf16[2,128,128]{1,2,0:T(8,128)(2,1)} collective-permute-done((bf16[2,128,128]{1,2,0:T(8,128)(2,1)S(1)}, bf16[2,128,128]{1,2,0:T(8,128)(2,1)}, u32[]{:S(2)}, u32[]{:S(2)}) %collective-permute-start.5) | collective-permute-done | bytes 65568 | tf_op jit(solution)/shard_map/ppermute | solution.py:114
  119.9 7.2 %collective-permute-done.6 = bf16[2,128,128]{1,2,0:T(8,128)(2,1)} collective-permute-done((bf16[2,128,128]{1,2,0:T(8,128)(2,1)}, bf16[2,128,128]{1,2,0:T(8,128)(2,1)}, u32[]{:S(2)}, u32[]{:S(2)}) %collective-permute-start.6) | collective-permute-done | bytes 65568 | tf_op jit(solution)/shard_map/ppermute | solution.py:114
  128.6 1.5 constant_dynamic-update-slice_fusion.16
  131.6 1.5 constant_dynamic-update-slice_fusion.14
  133.1 1.5 constant_dynamic-update-slice_fusion.13
  136.1 1.5 constant_dynamic-update-slice_fusion.11
  140.4 1.5 constant_dynamic-update-slice_fusion.7
  144.8 1.5 constant_dynamic-update-slice_fusion.4
  147.8 1.5 constant_dynamic-update-slice_fusion.2
  150.6 2.3 copy.58
  152.9 1.7 multiply_reduce_fusion.1
  154.9 22.4 %conditional.1 = ((f32[2,1,512]{2,0,1:T(2,128)S(1)}, f32[2,1,512,64]{2,3,0,1:T(8,128)S(1)})) conditional(s32[]{:T(128)} %convert_element_type.126, (f32[2,1,512]{2,0,1:T(2,128)S(1)}, f32[2,1,512,64]{2,3,0,1:T(8,128)S(1)}) %tuple.45, (s32[]{:T(128)}, s32[4,128]{1,0:T(4,128)S(1)}, s32[]{:T(128)}, s32[]{:T(128)}, bf16[2,2048,128]{1,2,0:T(8,128)(2,1)}, ...), branch_computations={%region_3.4_spmd, %region_4.0_spmd.clone} | conditional | flops 278534656 | bytes 50899244 | solution.py:163
  158.0 3.9 %sub.86 = f32[2,4,128,1024]{2,1,3,0:T(4,128)} broadcast(f32[2,4,1024]{1,2,0:T(8,128)S(1)} %copy.54), dimensions={0,1,3} | broadcast | bytes 4227072 | tf_op jit(solution)/shard_map/while/body/eval_jaxpr/cond/branch_1_fun/sub | solution.py:141
  161.9 5.5 %sub.87 = f32[2,512,1024]{1,2,0:T(8,128)} reshape(f32[2,4,128,1024]{2,1,3,0:T(4,128)} %sub.86) | data formatting | bytes 8388608 | tf_op jit(solution)/shard_map/while/body/eval_jaxpr/cond/branch_1_fun/sub | solution.py:141
  167.5 5.6 %fusion.77 = (f32[2,512]{1,0:T(2,128)S(1)}, f32[2,512,1024]{1,2,0:T(8,128)}) fusion(f32[2,512,1024]{1,2,0:T(8,128)} %sub.87, f32[2,512]{1,0:T(2,128)S(1)} %bitcast.187, bf16[2,512,64]{1,2,0:T(8,128)(2,1)S(1)} %reshape.387, bf16[2,2048,128]{1,2,0:T(8,128)(2,1)} %get-tuple-element.267, s32[]{:T(128)S(6)} %select_n.104, pred[512,1024]{0,1:T(8,128)(4,1)S(1)} %copy-done.4), kind=kOutput, calls=%fused_computation.186 | convolution fusion | flops 139459584 | bytes 9314308 | tf_op jit(solution)/shard_map/while/body/eval_jaxpr/cond/branch_1_fun/bhqd,bkhd->bhqk/dot_general | solution.py:135
  173.1 3.2 fusion.9
  177.8 1.7 convolution_convert_fusion
  187.1 2.0 convert_multiply_fusion
  189.1 1.6 slice.320
  190.7 1.6 slice.321
  193.7 1.8 multiply_add_fusion.1
  195.5 1.5 slice.326
  197.0 1.5 slice.327
  199.8 1.6 multiply_add_fusion.2
  243.1 1.5 slice.365
  247.2 1.6 slice.367
  260.2 1.5 fusion.57
  264.8 2.1 pad.129
  267.5 1.6 add.427
  269.1 1.7 fusion.53
  270.9 2.3 pad.118
  275.6 2.3 pad.132
  279.3 26.1 %all-gather = f32[16,1,256]{2,1,0:T(1,128)S(1)} all-gather(f32[2,1,256]{2,1,0:T(1,128)S(1)} %slice_add_fusion.4), channel_id=2, replica_groups=mesh['sp'=8,'tp'=4] {'sp'}, dimensions={0}, use_global_device_ids=true | all-gather | bytes 18432 | tf_op jit(solution)/shard_map/all_gather | solution.py:204
  305.4 26.1 %all-gather.1 = f32[16,1,256]{2,1,0:T(1,128)S(1)} all-gather(f32[2,1,256]{2,1,0:T(1,128)S(1)} %slice_add_fusion.3), channel_id=3, replica_groups=mesh['sp'=8,'tp'=4] {'sp'}, dimensions={0}, use_global_device_ids=true | all-gather | bytes 18432 | tf_op jit(solution)/shard_map/all_gather | solution.py:203
  332.0 3.0 fusion.82
  335.0 1.8 copy.71
  339.2 1.7 fusion.20
  342.0 22.1 %reduce-scatter.2.cloned.1.call-done = bf16[256,512]{1,0:T(8,128)(2,1)} async-done(((bf16[1024,512]{1,0:T(8,128)(2,1)}), bf16[256,512]{1,0:T(8,128)(2,1)}) %reduce-scatter.2.cloned.1.call-update) | async-done | bytes 262160 | tf_op jit(solution)/shard_map/reduce_scatter | solution.py:226
  (236 shorter events, 100.0 us)
Async XLA Ops:
  6.5 175.3 %copy-start = (bf16[256,2048]{1,0:T(8,128)(2,1)S(1)}, bf16[256,2048]{1,0:T(8,128)(2,1)}, u32[]{:S(2)}) copy-start(bf16[256,2048]{1,0:T(8,128)(2,1)} %param.38) | copy-start | bytes 3145732
  6.5 98.3 %copy-start.2 = (bf16[2,128,2048]{2,1,0:T(8,128)(2,1)S(1)}, bf16[2,128,2048]{2,1,0:T(8,128)(2,1)}, u32[]{:S(2)}) copy-start(bf16[2,128,2048]{2,1,0:T(8,128)(2,1)} %param.21) | copy-start | bytes 3145732
  6.5 98.3 %copy-start.11 = (f32[2048]{0:T(1024)S(1)}, f32[2048]{0:T(1024)}, u32[]{:S(2)}) copy-start(f32[2048]{0:T(1024)} %param.22) | copy-start | bytes 24580
  6.5 38.2 %copy-start.12 = (bf16[256,64]{0,1:T(8,128)(2,1)S(1)}, bf16[256,64]{0,1:T(8,128)(2,1)}, u32[]{:S(2)}) copy-start(bf16[256,64]{0,1:T(8,128)(2,1)} %param.24) | copy-start | bytes 98308
  6.5 69.6 %copy-start.16 = (f32[64]{0:T(128)S(1)}, f32[64]{0:T(128)}, u32[]{:S(2)}) copy-start(f32[64]{0:T(128)} %param.27) | copy-start | bytes 772
  6.5 144.1 %all-gather.6.cloned.1.call-start = ((), (), s32[]{:S(2)}) async-start(), calls=%async_computation.1 | async-start | bytes 1179648 | tf_op jit(solution)/shard_map/all_gather | solution.py:75
  7.3 170.5 %all-gather.8.cloned.1.call-start = ((), (), s32[]{:S(2)}) async-start(), calls=%async_computation.2 | async-start | bytes 1179648 | tf_op jit(solution)/shard_map/all_gather | solution.py:78
  8.0 323.9 %all-gather.10.cloned.1.call-start = ((), (), s32[]{:S(2)}) async-start(), calls=%async_computation.3 | async-start | bytes 1179648 | tf_op jit(solution)/shard_map/all_gather | solution.py:79
  9.6 103.0 %copy-start.15 = (bf16[4,256]{1,0:T(4,128)(2,1)S(1)}, bf16[4,256]{1,0:T(4,128)(2,1)}, u32[]{:S(2)}) copy-start(bf16[4,256]{1,0:T(4,128)(2,1)} %param.31) | copy-start | bytes 6148
  9.6 110.2 %copy-start.20 = (f32[256]{0:T(256)S(1)}, f32[256]{0:T(256)}, u32[]{:S(2)}) copy-start(f32[256]{0:T(256)} %param.34) | copy-start | bytes 3076
  76.2 7.1 %collective-permute-start = (bf16[2,128,128]{1,2,0:T(8,128)(2,1)S(1)}, bf16[2,128,128]{1,2,0:T(8,128)(2,1)S(1)}, u32[]{:S(2)}, u32[]{:S(2)}) collective-permute-start(bf16[2,128,128]{1,2,0:T(8,128)(2,1)S(1)} %pad_maximum_fusion.3), channel_id=1, source_target_pairs={{0,4},{4,8},{8,12},{12,16},{16,20},{20,24},{24,28},{28,0},{1,5},{5... | collective-permute-start | bytes 196616 | tf_op jit(solution)/shard_map/ppermute | solution.py:114
  83.3 36.5 %copy-start.5 = (bf16[2,128,128]{1,2,0:T(8,128)(2,1)}, bf16[2,128,128]{1,2,0:T(8,128)(2,1)S(1)}, u32[]{:S(2)}) copy-start(bf16[2,128,128]{1,2,0:T(8,128)(2,1)S(1)} %collective-permute-done) | copy-start | bytes 196612
  83.3 7.6 %collective-permute-start.1 = (bf16[2,128,128]{1,2,0:T(8,128)(2,1)S(1)}, bf16[2,128,128]{1,2,0:T(8,128)(2,1)S(1)}, u32[]{:S(2)}, u32[]{:S(2)}) collective-permute-start(bf16[2,128,128]{1,2,0:T(8,128)(2,1)S(1)} %collective-permute-done), channel_id=1, source_target_pairs={{0,4},{4,8},{8,12},{12,16},{16,20},{20,24},{24,28},{28,0},{1,5},{5... | collective-permute-start | bytes 196616 | tf_op jit(solution)/shard_map/ppermute | solution.py:114
  90.9 29.0 %copy-start.6 = (bf16[2,128,128]{1,2,0:T(8,128)(2,1)}, bf16[2,128,128]{1,2,0:T(8,128)(2,1)S(1)}, u32[]{:S(2)}) copy-start(bf16[2,128,128]{1,2,0:T(8,128)(2,1)S(1)} %collective-permute-done.1) | copy-start | bytes 196612
  90.9 7.0 %collective-permute-start.2 = (bf16[2,128,128]{1,2,0:T(8,128)(2,1)S(1)}, bf16[2,128,128]{1,2,0:T(8,128)(2,1)S(1)}, u32[]{:S(2)}, u32[]{:S(2)}) collective-permute-start(bf16[2,128,128]{1,2,0:T(8,128)(2,1)S(1)} %collective-permute-done.1), channel_id=1, source_target_pairs={{0,4},{4,8},{8,12},{12,16},{16,20},{20,24},{24,28},{28,0},{1,5},{5... | collective-permute-start | bytes 196616 | tf_op jit(solution)/shard_map/ppermute | solution.py:114
  97.9 22.0 %copy-start.7 = (bf16[2,128,128]{1,2,0:T(8,128)(2,1)}, bf16[2,128,128]{1,2,0:T(8,128)(2,1)S(1)}, u32[]{:S(2)}) copy-start(bf16[2,128,128]{1,2,0:T(8,128)(2,1)S(1)} %collective-permute-done.2) | copy-start | bytes 196612
  97.9 7.0 %collective-permute-start.3 = (bf16[2,128,128]{1,2,0:T(8,128)(2,1)S(1)}, bf16[2,128,128]{1,2,0:T(8,128)(2,1)S(1)}, u32[]{:S(2)}, u32[]{:S(2)}) collective-permute-start(bf16[2,128,128]{1,2,0:T(8,128)(2,1)S(1)} %collective-permute-done.2), channel_id=1, source_target_pairs={{0,4},{4,8},{8,12},{12,16},{16,20},{20,24},{24,28},{28,0},{1,5},{5... | collective-permute-start | bytes 196616 | tf_op jit(solution)/shard_map/ppermute | solution.py:114
  97.9 266.2 %reduce-scatter.2.cloned.1.call-start = ((), (), s32[]{:S(2)}) async-start(), calls=%async_computation.4 | async-start | bytes 1310720 | tf_op jit(solution)/shard_map/reduce_scatter | solution.py:226
  104.8 15.0 %copy-start.8 = (bf16[2,128,128]{1,2,0:T(8,128)(2,1)}, bf16[2,128,128]{1,2,0:T(8,128)(2,1)S(1)}, u32[]{:S(2)}) copy-start(bf16[2,128,128]{1,2,0:T(8,128)(2,1)S(1)} %collective-permute-done.3) | copy-start | bytes 196612
  104.9 7.1 %collective-permute-start.4 = (bf16[2,128,128]{1,2,0:T(8,128)(2,1)S(1)}, bf16[2,128,128]{1,2,0:T(8,128)(2,1)S(1)}, u32[]{:S(2)}, u32[]{:S(2)}) collective-permute-start(bf16[2,128,128]{1,2,0:T(8,128)(2,1)S(1)} %collective-permute-done.3), channel_id=1, source_target_pairs={{0,4},{4,8},{8,12},{12,16},{16,20},{20,24},{24,28},{28,0},{1,5},{5... | collective-permute-start | bytes 196616 | tf_op jit(solution)/shard_map/ppermute | solution.py:114
  106.2 46.7 %copy-start.3 = (bf16[2,128,2048]{2,1,0:T(8,128)(2,1)S(1)}, bf16[2,128,2048]{2,1,0:T(8,128)(2,1)}, u32[]{:S(2)}) copy-start(bf16[2,128,2048]{2,1,0:T(8,128)(2,1)} %multiply_convert_fusion) | copy-start | bytes 3145732
  106.2 48.4 %copy-start.21 = (f32[64]{0:T(128)S(1)}, f32[64]{0:T(128)}, u32[]{:S(2)}) copy-start(f32[64]{0:T(128)} %param.26) | copy-start | bytes 772
  111.9 0.6 copy-start.9
  112.5 7.3 %collective-permute-start.5 = (bf16[2,128,128]{1,2,0:T(8,128)(2,1)S(1)}, bf16[2,128,128]{1,2,0:T(8,128)(2,1)}, u32[]{:S(2)}, u32[]{:S(2)}) collective-permute-start(bf16[2,128,128]{1,2,0:T(8,128)(2,1)S(1)} %collective-permute-done.4), channel_id=1, source_target_pairs={{0,4},{4,8},{8,12},{12,16},{16,20},{20,24},{24,28},{28,0},{1,5},{5... | collective-permute-start | bytes 196616 | tf_op jit(solution)/shard_map/ppermute | solution.py:114
  119.8 7.3 %collective-permute-start.6 = (bf16[2,128,128]{1,2,0:T(8,128)(2,1)}, bf16[2,128,128]{1,2,0:T(8,128)(2,1)}, u32[]{:S(2)}, u32[]{:S(2)}) collective-permute-start(bf16[2,128,128]{1,2,0:T(8,128)(2,1)} %collective-permute-done.5), channel_id=1, source_target_pairs={{0,4},{4,8},{8,12},{12,16},{16,20},{20,24},{24,28},{28,0},{1,5},{5... | collective-permute-start | bytes 196616 | tf_op jit(solution)/shard_map/ppermute | solution.py:114
  161.9 5.6 %copy-start.4 = (pred[512,1024]{0,1:T(8,128)(4,1)S(1)}, pred[512,1024]{0,1:T(8,128)(4,1)}, u32[]{:S(2)}) copy-start(pred[512,1024]{0,1:T(8,128)(4,1)} %iota_compare_fusion) | copy-start | bytes 1572868 | tf_op jit(solution)/shard_map/while/body/eval_jaxpr/cond
  173.1 3.5 copy-start.1
  177.2 5.1 %copy-start.17 = (f32[1,256]{1,0:T(1,128)S(1)}, f32[1,256]{1,0:T(1,128)}, u32[]{:S(2)}) copy-start(f32[1,256]{1,0:T(1,128)} %get-tuple-element.344) | copy-start | bytes 3076
  177.2 5.1 %copy-start.18 = (f32[1,256]{1,0:T(1,128)S(1)}, f32[1,256]{1,0:T(1,128)}, u32[]{:S(2)}) copy-start(f32[1,256]{1,0:T(1,128)} %get-tuple-element.345) | copy-start | bytes 3076
  177.3 6.6 %copy-start.22 = (bf16[4,64,64]{2,1,0:T(8,128)(2,1)S(1)}, bf16[4,64,64]{2,1,0:T(8,128)(2,1)}, u32[]{:S(2)}) copy-start(bf16[4,64,64]{2,1,0:T(8,128)(2,1)} %param.32) | copy-start | bytes 98308
  179.5 2.8 collective-permute-start.7
  183.2 0.7 copy-start.10
  255.8 15.0 %copy-start.14 = (f32[2,1,256]{2,1,0:T(1,128)S(1)}, f32[2,1,256]{2,1,0:T(1,128)}, u32[]{:S(2)}) copy-start(f32[2,1,256]{2,1,0:T(1,128)} %slice.410) | copy-start | bytes 6148
  255.8 17.4 %copy-start.13 = (f32[2,1,256]{2,1,0:T(1,128)S(1)}, f32[2,1,256]{2,1,0:T(1,128)}, u32[]{:S(2)}) copy-start(f32[2,1,256]{2,1,0:T(1,128)} %slice.433) | copy-start | bytes 6148
  270.8 68.3 %copy-start.19 = (f32[256]{0:T(256)S(1)}, f32[256]{0:T(256)}, u32[]{:S(2)}) copy-start(f32[256]{0:T(256)} %param.37) | copy-start | bytes 3076
Sparse Core Ops, SparseCore 0:
  9.5 43.5 all-gather.5
  55.2 40.4 all-gather.7
  98.0 41.9 all-gather.9
  342.1 21.9 reduce-scatter.1
